TPU v7x, 32 devices: a whole 2x2x4 slice. The times are simulated.
32 devices in a mesh: kv: 8 (over z, core), tp: 4 (over y, x).
Axes of the slice: x: 2, y: 2, z: 4, core: 2. Of those that a mesh axis runs over, the one named last changes fastest.
Arguments:
- tokens: bfloat16 [24, 4096], P(None, 'kv'), may hold values from -24 to 24
- attention_norm_gain: float32 [4096], replicated, may hold values from 0.1 to 1.9
- query_weight: bfloat16 [4096, 2048], P('kv', 'tp'), may hold values from -0.09375 to 0.09375
- key_weight: bfloat16 [4096, 2048], P('kv', 'tp'), may hold values from -0.09375 to 0.09375
- value_weight: bfloat16 [4096, 4096], P('kv', 'tp'), may hold values from -0.09375 to 0.09375
- output_gate_weight: bfloat16 [4096, 4096], P('kv', 'tp'), may hold values from -0.09375 to 0.09375
- lowrank_weight: bfloat16 [4096, 16], replicated, may hold values from -0.09375 to 0.09375
- decay_weight: bfloat16 [16, 2048], replicated, may hold values from -1.5 to 1.5
- decay_preact_bias: float32 [2048], replicated, may hold values from -1 to 20
- head_norm_gain: float32 [256], replicated, may hold values from 0.1 to 1.9
- output_weight: bfloat16 [4096, 4096], P('tp', 'kv'), may hold values from -0.125 to 0.125
- feedforward_norm_gain: float32 [4096], replicated, may hold values from 0.1 to 1.9
- feedforward_gate_weight: bfloat16 [4096, 10240], P('kv', 'tp'), may hold values from -0.09375 to 0.09375
- feedforward_up_weight: bfloat16 [4096, 10240], P('kv', 'tp'), may hold values from -0.09375 to 0.09375
- feedforward_down_weight: bfloat16 [10240, 4096], P('tp', 'kv'), may hold values from -0.078125 to 0.078125
- past_key_cache: bfloat16 [24, 1536, 2048], P(None, 'kv', 'tp'), may hold values from -6 to 6
- past_value_cache: bfloat16 [24, 1536, 4096], P(None, 'kv', 'tp'), may hold values from -6 to 6
- past_lowrank_cache: bfloat16 [24, 16, 1536], P(None, None, 'kv'), may hold values from -8 to 8
- head_extra_decay: float32 [24, 16, 1536], P(None, 'tp', 'kv'), may hold values from -0.7 to 0
- lengths: int32 [24], replicated, may hold values from 1 to 1536, 10368 in all
Outputs:
- output: bfloat16 [24, 4096], P(None, 'kv')
All inputs are finite; a program needn't handle non-finite values.
Results may differ from a plain program's by a relative error of at most 0.0085.
Values may be sent and summed in bfloat16 or wider, within the bound.
A program may use at most 128 MiB of HBM per device.

v0:
```python
import jax
import jax.numpy as jnp
from jax import lax
from jax.sharding import PartitionSpec as P

D = 4096
KEY_CHANNELS = 128
DV = 256
BLOCK = 64


NORM_EPSILON = 1e-06


def product(operand, weights):
    return jnp.dot(operand, weights, preferred_element_type=jnp.float32)


def upper_ones(extent):
    row_ids = lax.broadcasted_iota(jnp.int32, (extent, extent), 0)
    col_ids = lax.broadcasted_iota(jnp.int32, (extent, extent), 1)
    return (col_ids > row_ids).astype(jnp.float32)


def shards(
    tokens,
    attention_norm_gain,
    query_weight,
    key_weight,
    value_weight,
    output_gate_weight,
    lowrank_weight,
    decay_weight,
    decay_preact_bias,
    head_norm_gain,
    output_weight,
    feedforward_norm_gain,
    feedforward_gate_weight,
    feedforward_up_weight,
    feedforward_down_weight,
    past_key_cache,
    past_value_cache,
    past_lowrank_cache,
    head_extra_decay,
    lengths,
):
    sequences, row_width = tokens.shape
    kv_index = lax.axis_index("kv")
    tp_index = lax.axis_index("tp")
    channels = query_weight.shape[1]
    device_heads = head_extra_decay.shape[1]
    positions = past_key_cache.shape[1]
    block_count = positions // BLOCK
    row_start = kv_index * row_width
    rows_float = tokens.astype(jnp.float32)
    gain_one = lax.dynamic_slice_in_dim(attention_norm_gain, row_start, row_width)
    scaled = (rows_float * gain_one).astype(jnp.bfloat16)
    low_rows = lax.dynamic_slice_in_dim(lowrank_weight, row_start, row_width, 0)
    projected = lax.psum(
        (
            jnp.sum(rows_float * rows_float, axis=1),
            product(scaled, query_weight),
            product(scaled, key_weight),
            product(scaled, value_weight),
            product(scaled, output_gate_weight),
            product(scaled, low_rows),
        ),
        "kv",
    )
    sq_total, query_part, key_part, value_part, outgate_part, lowrank_part = projected
    inv_rms = lax.rsqrt(sq_total / D + NORM_EPSILON)[:, None]
    query_vector = (inv_rms * query_part).astype(jnp.bfloat16)
    fresh_key = (inv_rms * key_part).astype(jnp.bfloat16)
    fresh_value = (inv_rms * value_part).astype(jnp.bfloat16)
    outgate = (inv_rms * outgate_part).astype(jnp.bfloat16)
    lowrank = (inv_rms * lowrank_part).astype(jnp.bfloat16)
    chan_start = tp_index * channels
    decay_cols = lax.dynamic_slice_in_dim(decay_weight, chan_start, channels, 1)
    bias_cols = lax.dynamic_slice_in_dim(decay_preact_bias, chan_start, channels)
    fresh_gate_value = jax.nn.log_sigmoid(product(lowrank, decay_cols) + bias_cols) / 16.0
    pre_cache = (
        jnp.einsum(
            "srp,rc->spc", past_lowrank_cache, decay_cols, preferred_element_type=jnp.float32
        )
        + bias_cols
    )
    gate_cache = jax.nn.log_sigmoid(pre_cache) / 16.0
    gate_cache = (
        gate_cache.reshape(sequences, positions, device_heads, KEY_CHANNELS)
        + jnp.transpose(head_extra_decay, (0, 2, 1))[..., None]
    )
    position_ids = kv_index * positions + lax.broadcasted_iota(jnp.int32, (sequences, positions), 1)
    is_live = position_ids < lengths[:, None]
    gate_cache = jnp.where(is_live[:, :, None, None], gate_cache, 0.0).reshape(
        sequences, block_count, BLOCK, channels
    )
    inside = jnp.einsum(
        "ij,snjc->snic", upper_ones(BLOCK), gate_cache, precision=lax.Precision.HIGHEST
    )
    block_totals = jnp.sum(gate_cache, axis=2)
    after_blocks = jnp.einsum(
        "mn,snc->smc", upper_ones(block_count), block_totals, precision=lax.Precision.HIGHEST
    )
    local_total = jnp.sum(block_totals, axis=1)
    pieces = lax.all_gather(local_total[:, None, :], "kv", axis=1, tiled=True)
    beyond = lax.broadcasted_iota(jnp.int32, (1, pieces.shape[1], 1), 1) > kv_index
    later_sum = jnp.sum(jnp.where(beyond, pieces, 0.0), axis=1)
    carried = after_blocks + later_sum[:, None, :] + fresh_gate_value[:, None, :]
    weighting = jnp.exp(inside + carried[:, :, None, :]).reshape(sequences, positions, channels)
    query_scaled = query_vector.astype(jnp.float32) * KEY_CHANNELS ** (-0.5)
    products = past_key_cache.astype(jnp.float32) * weighting * query_scaled[:, None, :]
    scores = jnp.sum(products.reshape(sequences, positions, device_heads, KEY_CHANNELS), axis=3)
    scores = jnp.where(is_live[:, :, None], scores, 0.0).astype(jnp.bfloat16)
    partial_out = jnp.einsum(
        "sph,sphv->shv",
        scores,
        past_value_cache.reshape(sequences, positions, device_heads, DV),
        preferred_element_type=jnp.float32,
    )
    summed = lax.psum(partial_out, "kv")
    own_score = jnp.sum(
        (query_scaled * fresh_key.astype(jnp.float32)).reshape(
            sequences, device_heads, KEY_CHANNELS
        ),
        axis=2,
    )
    mixer_output = summed + own_score[:, :, None] * fresh_value.astype(jnp.float32).reshape(
        sequences, device_heads, DV
    )
    mean_sq = jnp.mean(mixer_output * mixer_output, axis=2, keepdims=True)
    gate_act = jax.nn.silu(outgate.astype(jnp.float32).reshape(sequences, device_heads, DV))
    gated = (mixer_output * lax.rsqrt(mean_sq + NORM_EPSILON) * head_norm_gain * gate_act).astype(
        jnp.bfloat16
    )
    attn_rows = lax.psum(product(gated.reshape(sequences, device_heads * DV), output_weight), "tp")
    residual = rows_float + attn_rows
    gain_two = lax.dynamic_slice_in_dim(feedforward_norm_gain, row_start, row_width)
    scaled_two = (residual * gain_two).astype(jnp.bfloat16)
    square_two = jnp.sum(residual * residual, axis=1)
    sq_sum, gate_sum, up_sum = lax.psum(
        (
            square_two,
            product(scaled_two, feedforward_gate_weight),
            product(scaled_two, feedforward_up_weight),
        ),
        "kv",
    )
    inv_two = lax.rsqrt(sq_sum / D + NORM_EPSILON)[:, None]
    hidden = (jax.nn.silu(inv_two * gate_sum) * (inv_two * up_sum)).astype(jnp.bfloat16)
    down_part = product(hidden, feedforward_down_weight)
    mlp_rows = lax.psum(down_part, "tp")
    return (residual + mlp_rows).astype(jnp.bfloat16)


def solution(mesh):
    return jax.shard_map(
        shards,
        mesh=mesh,
        in_specs=(
            P(None, "kv"),
            P(),
            P("kv", "tp"),
            P("kv", "tp"),
            P("kv", "tp"),
            P("kv", "tp"),
            P(),
            P(),
            P(),
            P(),
            P("tp", "kv"),
            P(),
            P("kv", "tp"),
            P("kv", "tp"),
            P("tp", "kv"),
            P(None, "kv", "tp"),
            P(None, "kv", "tp"),
            P(None, None, "kv"),
            P(None, "tp", "kv"),
            P(),
        ),
        out_specs=P(None, "kv"),
        check_vma=False,
    )
```

profile of v0, /device:TPU:0, one launch (start us, length us, event | category | flops | bytes accessed | tf_op | source)
XLA Modules:
  0.0 302.4 jit_solution(8154812676374695162)
XLA Ops:
  6.5 1.6 fusion.22
  10.4 1.9 fusion.39
  12.2 1.9 fusion.41
  14.2 3.1 %copy.23 = f32[24,192,4]{2,1,0:T(8,128)} copy(f32[24,192,4]{1,2,0:T(4,128)} %bitcast.81) | data formatting | bytes 147456 | tf_op jit(solution)/shard_map/transpose | solution.py:90
  17.2 7.6 %add.160 = f32[24,192,4,128]{3,2,1,0:T(4,128)} broadcast(f32[24,192,4]{2,1,0:T(8,128)} %copy.23), dimensions={0,1,2} | broadcast | bytes 9510912 | tf_op jit(solution)/shard_map/add | solution.py:89
  24.8 12.3 %add.163 = f32[24,192,512]{2,1,0:T(8,128)} reshape(f32[24,192,4,128]{3,2,1,0:T(4,128)} %add.160) | data formatting | bytes 18874368 | tf_op jit(solution)/shard_map/add | solution.py:89
  37.1 12.4 %add.161 = f32[24,3,64,512]{3,2,1,0:T(8,128)} reshape(f32[24,192,4,128]{3,2,1,0:T(4,128)} %add.160) | data formatting | bytes 18874368 | tf_op jit(solution)/shard_map/add | solution.py:89
  50.6 10.3 %select_reduce_fusion = (f32[24,512]{1,0:T(8,128)S(1)}, f32[24,192,512]{2,1,0:T(8,128)S(1)}) fusion(f32[24,192,512]{2,1,0:T(8,128)} %add.163, pred[24,192]{1,0:T(8,128)(4,1)S(1)} %broadcast_compare_fusion.1, f32[512]{0:T(512)S(1)} %dynamic_slice.16, bf16[24,16,192]{2,1,0:T(8,128)(2,1)S(1)} %copy-done.9, bf16[16,2048]{1,0:T(8,128)(2,1)S(1)} %copy-done.10, ...), kind=kOutput, calls=%fused_computation.15 | convolution fusion | flops 106156032 | bytes 19144708 | tf_op jit(solution)/shard_map/srp,rc->spc/dot_general | solution.py:82
  61.0 16.3 %all-gather = f32[24,4096]{1,0:T(8,128)S(1)} all-gather(f32[24,512]{1,0:T(8,128)S(1)} %get-tuple-element.20), channel_id=2, replica_groups=mesh['kv'=8,'tp'=4] {'kv'}, dimensions={1}, use_global_device_ids=true | all-gather | bytes 442368 | tf_op jit(solution)/shard_map/all_gather | solution.py:105
  79.3 2.4 fusion.10
  83.9 14.2 %add_exponential_fusion = f32[24,3,512,64]{2,3,1,0:T(8,128)} fusion(f32[24,3,512]{2,1,0:T(4,128)S(1)} %fusion.14, f32[24,3,64,512]{3,2,1,0:T(8,128)} %bitcast.73, f32[24,3,64,512]{3,2,1,0:T(8,128)} %add.161, pred[24,3,64]{2,1,0:T(4,128)(4,1)S(1)} %broadcast_compare_fusion), kind=kOutput, calls=%fused_computation.14 | convolution fusion | flops 1819021312 | bytes 28463616 | tf_op jit(solution)/shard_map/ij,snjc->snic/dot_general | solution.py:97
  98.2 9.4 %fusion.5 = f32[24,192,512]{2,1,0:T(8,128)} fusion(f32[24,3,512,64]{2,3,1,0:T(8,128)} %add_exponential_fusion, bf16[24,192,512]{2,1,0:T(8,128)(2,1)S(1)} %bitcast.76, f32[24,512]{1,0:T(8,128)S(1)} %get-tuple-element.17), kind=kLoop, calls=%fused_computation.7 | loop fusion | flops 7077888 | bytes 23642112 | tf_op jit(solution)/shard_map/mul | solution.py:111
  107.6 11.9 %reshape.121 = f32[24,192,4,128]{3,2,1,0:T(4,128)} reshape(f32[24,192,512]{2,1,0:T(8,128)} %fusion.5) | data formatting | bytes 18874368 | tf_op jit(solution)/shard_map/reshape | solution.py:112
  119.5 9.9 %reduce_sum.76 = bf16[24,192,4]{2,1,0:T(8,128)(2,1)} reduce(f32[24,192,4,128]{3,2,1,0:T(4,128)} %reshape.121, f32[]{:T(128)} %constant.43.clone.1), dimensions={3}, to_apply=%region_7.8 | reduce | flops 2340864 | bytes 9474052 | tf_op jit(solution)/shard_map/reduce_sum | solution.py:112
  129.4 3.4 %fusion.12 = bf16[24,192,4,1]{2,1,0,3:T(8,128)(2,1)} fusion(bf16[24,192,4]{2,1,0:T(8,128)(2,1)} %reduce_sum.76, pred[24,192]{1,0:T(8,128)(4,1)S(1)} %broadcast_compare_fusion.1), kind=kLoop, calls=%fused_computation.20 | loop fusion | flops 18432 | bytes 78336 | tf_op jit(solution)/shard_map/convert_element_type | solution.py:113
  132.8 2.3 copy.25
  135.1 5.0 %fusion.2 = f32[24,4,1,256]{3,2,1,0:T(1,128)S(1)} fusion(bf16[24,192,4,1]{1,3,2,0:T(2,128)(2,1)S(1)} %copy.25, bf16[24,24,4,8,256]{4,3,2,1,0:T(8,128)(2,1)} %bitcast.74), kind=kOutput, calls=%fused_computation.3 | convolution fusion | flops 9437184 | bytes 9572352 | tf_op jit(solution)/shard_map/sph,sphv->shv/dot_general | solution.py:114
  141.8 53.7 %all-reduce.11.cloned.1.call-done = (f32[24,1024]{1,0:T(8,128)}, f32[24,4,256]{2,1,0:T(4,128)}, f32[24,1024]{1,0:T(8,128)}) async-done(((f32[24,1024]{1,0:T(8,128)}, f32[24,4,256]{2,1,0:T(4,128)}, f32[24,1024]{1,0:T(8,128)}), (f32[24,1024]{1,0:T(8,128)}, f32[24,4,256]{2,1,0:T(4,128)}, f32[24,1024]{1,0:T(8,128)})) %all-reduce.11.cloned.1.call-update) | async-done | bytes 294928 | tf_op jit(solution)/shard_map/psum | solution.py:59
  200.3 16.8 %psum.91 = f32[24,512]{1,0:T(8,128)S(1)} all-reduce(f32[24,512]{1,0:T(8,128)S(1)} %fusion.52), channel_id=1, replica_groups=mesh['kv'=8,'tp'=4] {'tp'}, use_global_device_ids=true, to_apply=%region_14.15 | all-reduce | flops 12288 | bytes 98304 | tf_op jit(solution)/shard_map/psum | solution.py:135
  218.3 2.9 fusion.54
  221.2 13.6 %psum.92 = f32[24]{0:T(128)S(1)} all-reduce(f32[24]{0:T(128)S(1)} %get-tuple-element.14), channel_id=1, replica_groups=mesh['kv'=8,'tp'=4] {'kv'}, use_global_device_ids=true, to_apply=%region_16.17 | all-reduce | flops 24 | bytes 192 | tf_op jit(solution)/shard_map/psum | solution.py:140
  234.8 41.2 %all-reduce.9.cloned.1.call-done = (f32[24,2560]{1,0:T(8,128)}, f32[24,2560]{1,0:T(8,128)}) async-done(((f32[24,2560]{1,0:T(8,128)}, f32[24,2560]{1,0:T(8,128)}), (f32[24,2560]{1,0:T(8,128)}, f32[24,2560]{1,0:T(8,128)})) %all-reduce.9.cloned.1.call-update) | async-done | bytes 491536 | tf_op jit(solution)/shard_map/psum | solution.py:140
  276.1 2.5 fusion.17
  278.6 16.7 %psum.95 = f32[24,512]{1,0:T(8,128)S(1)} all-reduce(f32[24,512]{1,0:T(8,128)S(1)} %fusion.17), channel_id=1, replica_groups=mesh['kv'=8,'tp'=4] {'tp'}, use_global_device_ids=true, to_apply=%region_19.20 | all-reduce | flops 12288 | bytes 98304 | tf_op jit(solution)/shard_map/psum | solution.py:151
  (73 shorter events, 15.9 us)
Async XLA Ops:
  6.5 210.6 %copy-start = (bf16[512,2560]{1,0:T(8,128)(2,1)S(1)}, bf16[512,2560]{1,0:T(8,128)(2,1)}, u32[]{:S(2)}) copy-start(bf16[512,2560]{1,0:T(8,128)(2,1)} %param.32) | copy-start | bytes 7864324
  6.5 75.4 %all-reduce.7.cloned.1.call-start = ((), (), s32[]{:S(2)}) async-start(), calls=%async_computation | async-start | bytes 214016 | tf_op jit(solution)/shard_map/psum | solution.py:59
  14.1 181.4 %all-reduce.11.cloned.1.call-start = ((), (), s32[]{:S(2)}) async-start(), calls=%async_computation.2 | async-start | bytes 589824 | tf_op jit(solution)/shard_map/psum | solution.py:59
  37.1 12.4 %copy-start.7 = (s32[24]{0:T(128)S(1)}, s32[24]{0:T(128)}, u32[]{:S(2)}) copy-start(s32[24]{0:T(128)} %param.39) | copy-start | bytes 292
  37.1 13.5 %copy-start.9 = (bf16[24,16,192]{2,1,0:T(8,128)(2,1)S(1)}, bf16[24,16,192]{2,1,0:T(8,128)(2,1)}, u32[]{:S(2)}) copy-start(bf16[24,16,192]{2,1,0:T(8,128)(2,1)} %param.37) | copy-start | bytes 442372
  37.1 13.5 %copy-start.10 = (bf16[16,2048]{1,0:T(8,128)(2,1)S(1)}, bf16[16,2048]{1,0:T(8,128)(2,1)}, u32[]{:S(2)}) copy-start(bf16[16,2048]{1,0:T(8,128)(2,1)} %param.27) | copy-start | bytes 196612
  49.7 29.6 %slice-start = ((s8[9437184]{0:T(1024)(128)(4,1)}), s8[4194304]{0:T(1024)(128)(4,1)S(1)}, s32[]{:S(2)}) async-start(s8[9437184]{0:T(1024)(128)(4,1)} %bitcast.70), calls=%async_computation.3 | async-start | bytes 8388608
  50.6 26.9 %copy-start.2 = (bf16[24,512]{1,0:T(8,128)(2,1)S(1)}, bf16[24,512]{1,0:T(8,128)(2,1)}, u32[]{:S(2)}) copy-start(bf16[24,512]{1,0:T(8,128)(2,1)} %param.20) | copy-start | bytes 73732
  50.6 26.9 %copy-start.3 = (bf16[512,1024]{1,0:T(8,128)(2,1)S(1)}, bf16[512,1024]{1,0:T(8,128)(2,1)}, u32[]{:S(2)}) copy-start(bf16[512,1024]{1,0:T(8,128)(2,1)} %param.25) | copy-start | bytes 3145732
  50.6 27.8 %copy-start.4 = (bf16[512,1024]{1,0:T(8,128)(2,1)S(1)}, bf16[512,1024]{1,0:T(8,128)(2,1)}, u32[]{:S(2)}) copy-start(bf16[512,1024]{1,0:T(8,128)(2,1)} %param.24) | copy-start | bytes 3145732
  50.6 28.7 %slice-start.1 = ((s8[9437184]{0:T(1024)(128)(4,1)}), s8[4194304]{0:T(1024)(128)(4,1)S(1)}, s32[]{:S(2)}) async-start(s8[9437184]{0:T(1024)(128)(4,1)} %bitcast.70), calls=%async_computation.4 | async-start | bytes 8388608
  50.6 28.7 %slice-start.2 = ((s8[9437184]{0:T(1024)(128)(4,1)}), s8[1048576]{0:T(1024)(128)(4,1)S(1)}, s32[]{:S(2)}) async-start(s8[9437184]{0:T(1024)(128)(4,1)} %bitcast.70), calls=%async_computation.5 | async-start | bytes 2097152
  61.0 20.8 %copy-start.1 = (f32[24,192,512]{2,1,0:T(8,128)}, f32[24,192,512]{2,1,0:T(8,128)S(1)}, u32[]{:S(2)}) copy-start(f32[24,192,512]{2,1,0:T(8,128)S(1)} %get-tuple-element.21) | copy-start | bytes 28311556
  79.3 18.9 %slice-start.3 = ((s8[4718592]{0:T(1024)(128)(4,1)}), s8[524288]{0:T(1024)(128)(4,1)S(1)}, s32[]{:S(2)}) async-start(s8[4718592]{0:T(1024)(128)(4,1)} %bitcast.75), calls=%async_computation.6 | async-start | bytes 1048576
  83.8 14.2 %copy-start.5 = (f32[24,512]{1,0:T(8,128)S(1)}, f32[24,512]{1,0:T(8,128)}, u32[]{:S(2)}) copy-start(f32[24,512]{1,0:T(8,128)} %get-tuple-element.7) | copy-start | bytes 147460
  83.9 14.2 %copy-start.6 = (f32[24,512]{1,0:T(8,128)S(1)}, f32[24,512]{1,0:T(8,128)}, u32[]{:S(2)}) copy-start(f32[24,512]{1,0:T(8,128)} %get-tuple-element.8) | copy-start | bytes 147460
  83.9 14.3 %slice-start.4 = ((s8[4718592]{0:T(1024)(128)(4,1)}), s8[4194304]{0:T(1024)(128)(4,1)S(1)}, s32[]{:S(2)}) async-start(s8[4718592]{0:T(1024)(128)(4,1)} %bitcast.75), calls=%async_computation.7 | async-start | bytes 8388608
  129.4 68.4 %copy-start.8 = (f32[256]{0:T(256)S(1)}, f32[256]{0:T(256)}, u32[]{:S(2)}) copy-start(f32[256]{0:T(256)} %param.29) | copy-start | bytes 3076
  140.9 135.2 %all-reduce.9.cloned.1.call-start = ((), (), s32[]{:S(2)}) async-start(), calls=%async_computation.1 | async-start | bytes 983040 | tf_op jit(solution)/shard_map/psum | solution.py:140
Sparse Core Ops, SparseCore 0:
  14.2 55.5 all-reduce.6
  141.0 54.4 all-reduce.10
  221.3 54.6 all-reduce.8
where the time goes:
time: 304 us; the launch traced here: 302 us
  waiting for transfers between devices  95 us (31%)
  blocking collectives  63.3 us (21%)
  local copies, waits for them, and re-layouts  53.1 us (17%)
  matrix products  45.8 us (15%)
  other arithmetic  31.8 us (10%)
  between operations  13.4 us (4%)
    psum x2, waiting for transfers between devices, shards(): lax.psum((jnp.sum(rows_float * rows_float, axis=1), product(scaled, query...  53.7 us
    psum x1, waiting for transfers between devices, shards(): lax.psum((square_two, product(scaled_two, feedforward_gate_weight), produ...  41.2 us
    add x3, local copies, waits for them, and re-layouts, shards(): gate_cache.reshape(sequences, positions, device_heads, KEY_CHANNELS)  32.2 us
    psum x1, blocking collectives, shards(): lax.psum(product(gated.reshape(sequences, device_heads * DV), output_weig...  16.8 us
    psum x1, blocking collectives, shards(): mlp_rows = lax.psum(down_part, 'tp')  16.7 us
    all_gather x1, blocking collectives, shards(): pieces = lax.all_gather(local_total[:, None, :], 'kv', axis=1, tiled=True)  16.3 us
    dot_general x10, matrix products, product(): return jnp.dot(operand, weights, preferred_element_type=jnp.float32)  15.9 us
    dot_general x1, matrix products, shards(): jnp.einsum('ij,snjc->snic', upper_ones(BLOCK), gate_cache, precision=lax....  14.2 us
  transfers between devices with their start and end apart: 3, of which 2 were waited for; matrix products, arithmetic and copies ran while one was open for 17% of the time, Pallas kernels for 0%

commit v1 on v0

v1 whole, which is shorter than its diff:
```python
import functools

import jax
import jax.numpy as jnp
from jax import lax
from jax.experimental import pallas as pl
from jax.experimental.pallas import tpu as pltpu
from jax.sharding import PartitionSpec as P

NORM_EPSILON = 1e-06
LANES = 128
CHUNK = 512
F32 = jnp.float32
BF16 = jnp.bfloat16


def dot(a, b):
    return jnp.dot(a, b, preferred_element_type=F32)


def log_sigmoid(v):
    return jnp.minimum(v, 0.0) - jnp.log(1.0 + jnp.exp(-jnp.abs(v)))


def remote(src, dst, send_sem, recv_sem, axis, dest):
    return pltpu.make_async_remote_copy(
        src_ref=src,
        dst_ref=dst,
        send_sem=send_sem,
        recv_sem=recv_sem,
        device_id={axis: dest},
        device_id_type=pl.DeviceIdType.MESH,
    )


class Exchange:
    def __init__(self, axis, size, out, slots, send_sem, recv_sem, same=False):
        self.axis, self.size, self.out, self.slots = axis, size, out, slots
        self.send_sem, self.recv_sem, self.same = send_sem, recv_sem, same
        self.me = lax.axis_index(axis)

    def source(self, dest):
        return self.out if self.same else self.out.at[dest]

    def to(self, dest):
        return remote(
            self.source(dest), self.slots.at[self.me], self.send_sem.at[dest],
            self.recv_sem.at[self.me], self.axis, dest,
        )

    def start(self):
        for k in range(1, self.size):
            self.to(lax.rem(self.me + k, self.size)).start()

    def arrived(self, origin):
        remote(
            self.source(origin), self.slots.at[origin], self.send_sem.at[origin],
            self.recv_sem.at[origin], self.axis, origin,
        ).wait_recv()

    def wait_recv(self):
        for k in range(1, self.size):
            self.arrived(lax.rem(self.me + k, self.size))

    def wait_send(self):
        for k in range(1, self.size):
            self.to(lax.rem(self.me + k, self.size)).wait_send()


def layer(
    n, m, spd,
    tokens_h, gain1_h, wq_h, wk_h, wv_h, wo_h, low_h, dw_h, bias_h, hgain_h, wout_h,
    gain2_h, wg_h, wu_h, wd_h, key_h, val_h, lr_h, ext_h, len_ref,
    out_ref,
    tokens, gain1, wq, wk, wv, wo, low, dw, bias, hgain, wout, gain2, wg, wu, wd,
    key, val, lr, ext,
    tri, tri_t, efac, a_full, a_send, a_recv, t_send, t_recv, q_send, q_recv,
    p_send, p_recv, g_own, g_recv, g_full, o_own, o_recv, s_own, s_recv,
    e_send, e_recv, h_own, h_recv, f_own, f_recv,
    in_sem, key_sem, val_sem, kv_ss, kv_rs, tp_ss, tp_rs,
):
    me = lax.axis_index("kv")
    mt = lax.axis_index("tp")
    seqs, width = tokens.shape
    chans, vals = wq.shape[1], wv.shape[1]
    heads, positions = ext.shape[1], ext.shape[2]
    kc, dv = chans // heads, vals // heads
    rank = low.shape[1]
    hidden = wg.shape[1]
    hw = e_send.shape[2]
    model = width * n

    def rows_of(ref, start, size):
        return ref.at[pl.ds(pl.multiple_of(start, size), size)]

    def cols_of(ref, start, size):
        return ref.at[:, pl.ds(pl.multiple_of(start, size), size)]

    sources = [
        (tokens_h, tokens),
        (cols_of(gain1_h, me * width, width), gain1),
        (wq_h, wq), (wk_h, wk), (wv_h, wv), (wo_h, wo),
        (rows_of(low_h, me * width, width), low),
        (cols_of(dw_h, mt * chans, chans), dw),
        (cols_of(bias_h, mt * chans, chans), bias),
        (lr_h, lr), (ext_h, ext),
    ]
    later = [
        (hgain_h, hgain), (wout_h, wout),
        (cols_of(gain2_h, me * width, width), gain2),
        (wg_h, wg), (wu_h, wu), (wd_h, wd),
    ]
    fetch = [pltpu.make_async_copy(a, b, in_sem.at[i]) for i, (a, b) in enumerate(sources + later)]
    for c in fetch[:len(sources)]:
        c.start()

    def key_copy(s):
        return pltpu.make_async_copy(key_h.at[s], key.at[s], key_sem.at[s])

    def val_copy(s):
        return pltpu.make_async_copy(val_h.at[s], val.at[s], val_sem.at[s])

    pl.loop(0, seqs)(lambda s: key_copy(s).start())
    pl.loop(0, seqs)(lambda s: val_copy(s).start())
    for c in fetch[len(sources):]:
        c.start()

    barrier = pltpu.get_barrier_semaphore()
    for axis, size, own in (("kv", n, me), ("tp", m, mt)):
        for k in range(1, size):
            pl.semaphore_signal(
                barrier, inc=1, device_id={axis: lax.rem(own + k, size)},
                device_id_type=pl.DeviceIdType.MESH,
            )

    def kv_exchange(i, out, slots, same=False):
        return Exchange("kv", n, out, slots, kv_ss.at[i], kv_rs.at[i], same)

    def tp_exchange(i, out, slots):
        return Exchange("tp", m, out, slots, tp_ss.at[i], tp_rs.at[i], True)

    ax = kv_exchange(0, a_send, a_recv)
    tx = kv_exchange(1, t_send, t_recv)
    qx = kv_exchange(2, q_send, q_recv)
    px = kv_exchange(3, p_send, p_recv)
    gx = kv_exchange(4, g_own, g_recv, True)
    sx = kv_exchange(5, s_own, s_recv, True)
    ex = kv_exchange(6, e_send, e_recv)
    hx = kv_exchange(7, h_own, h_recv, True)
    ox = tp_exchange(0, o_own, o_recv)
    fx = tp_exchange(1, f_own, f_recv)

    row = lax.broadcasted_iota(jnp.int32, tri.shape, 0)
    col = lax.broadcasted_iota(jnp.int32, tri.shape, 1)
    tri[...] = jnp.where((col > row) | (row >= positions), 1.0, 0.0).astype(BF16)
    row = lax.broadcasted_iota(jnp.int32, tri_t.shape, 0)
    col = lax.broadcasted_iota(jnp.int32, tri_t.shape, 1)
    tri_t[...] = jnp.where(row > col, 1.0, 0.0).astype(BF16)

    fetch[0].wait()
    fetch[1].wait()
    rows_float = tokens[...].astype(F32)
    scaled = (rows_float * gain1[...]).astype(BF16)
    base = 0
    for i, w in enumerate((wq, wk, wv, wo)):
        fetch[2 + i].wait()
        step = min(CHUNK, w.shape[1])
        for c in range(0, w.shape[1], step):
            a_full[:, base + c:base + c + step] = dot(scaled, w[:, c:c + step])
        base += w.shape[1]
    low_at, sq_at = base, base + LANES
    fetch[6].wait()
    a_full[:, low_at:low_at + LANES] = jnp.zeros((seqs, LANES), F32)
    a_full[:, low_at:low_at + rank] = dot(scaled, low[...])
    a_full[:, sq_at:sq_at + LANES] = jnp.broadcast_to(
        jnp.sum(rows_float * rows_float, axis=1, keepdims=True), (seqs, LANES)
    )
    for d in range(min(n, seqs // spd)):
        a_send[d] = a_full[d * spd:(d + 1) * spd, :]
    pl.semaphore_wait(barrier, n + m - 2)
    ax.start()
    a_recv[me] = a_send[me]

    for i in range(7, 11):
        fetch[i].wait()
    spot = me * positions
    head_of = lax.broadcasted_iota(jnp.int32, (heads, chans), 1) // kc
    head_row = lax.broadcasted_iota(jnp.int32, (heads, chans), 0)

    def decays(g, i):
        s = g * spd + i
        length = len_ref[s]
        pre = lax.dot_general(
            lr[s], dw[...], (((0,), (0,)), ((), ())), preferred_element_type=F32
        ) + bias[...]
        gate = log_sigmoid(pre) * (1.0 / 16.0)
        at = spot + lax.broadcasted_iota(jnp.int32, gate.shape, 0)
        gate = jnp.where(at < length, gate, 0.0)
        high = gate.astype(BF16)
        rest = (gate - high.astype(F32)).astype(BF16)
        suffix = dot(tri[...], high) + dot(tri[...], rest)
        weighting = jnp.exp(suffix[:positions])
        key_copy(s).wait()
        key[s] = (key[s].astype(F32) * weighting).astype(BF16)
        at = spot + lax.broadcasted_iota(jnp.int32, (heads, positions), 1)
        extra = jnp.where(at < length, ext[s], 0.0)
        high = extra.astype(BF16)
        rest = (extra - high.astype(F32)).astype(BF16)
        beyond = dot(high, tri_t[...]) + dot(rest, tri_t[...])
        efac[s, 0:heads, :] = jnp.where(at < length, jnp.exp(beyond), 0.0)
        if heads < 8:
            efac[s, heads:8, :] = jnp.zeros((8 - heads, positions), F32)
        whole = jnp.sum(extra, axis=1, keepdims=True)
        spread = jnp.sum(jnp.where(head_of == head_row, whole, 0.0), axis=0, keepdims=True)
        t_send[g, i:i + 1, :] = suffix[positions:positions + 1] + spread

    def guarded(body, g):
        for i in range(spd):
            if n * spd == seqs:
                body(g, i)
            else:
                pl.when(g * spd + i < seqs)(functools.partial(body, g, i))

    @pl.loop(0, n)
    def _(g):
        guarded(decays, g)

        @pl.when(g != me)
        def _():
            tx.to(g).start()

        @pl.when(g == me)
        def _():
            t_recv[me] = t_send[g]

    ax.wait_recv()
    total = a_recv[0]
    for e in range(1, n):
        total = total + a_recv[e]
    inv = lax.rsqrt(total[:, sq_at:sq_at + 1] / model + NORM_EPSILON)

    def rounded(start, size):
        return (inv * total[:, start:start + size]).astype(BF16)

    query = rounded(0, chans).astype(F32) * kc ** (-0.5)
    fresh_key = rounded(chans, chans).astype(F32)
    fresh_value = rounded(2 * chans, vals).astype(F32)
    outgate = rounded(2 * chans + vals, vals).astype(F32)
    fresh_gate = log_sigmoid(dot(rounded(low_at, rank), dw[...]) + bias[...]) * (1.0 / 16.0)
    qk = query * fresh_key
    tx.wait_recv()
    beyond = fresh_gate
    for e in range(n - 1, -1, -1):
        q_send[e] = query * jnp.exp(beyond)
        beyond = beyond + t_recv[e]
    qx.start()
    q_recv[me] = q_send[me]

    q_head = lax.broadcasted_iota(jnp.int32, (8, chans), 1) // kc
    q_row = lax.broadcasted_iota(jnp.int32, (8, chans), 0)
    v_head = lax.broadcasted_iota(jnp.int32, (8, vals), 1) // dv
    v_row = lax.broadcasted_iota(jnp.int32, (8, vals), 0)

    def mix(g, i):
        s = g * spd + i
        queries = jnp.where(q_head == q_row, q_recv[g, i:i + 1, :], 0.0).astype(BF16)
        scores = lax.dot_general(
            queries, key[s], (((1,), (1,)), ((), ())), preferred_element_type=F32
        ) * efac[s]
        val_copy(s).wait()
        sums = dot(scores.astype(BF16), val[s])
        p_send[g, i:i + 1, :] = jnp.sum(jnp.where(v_head == v_row, sums, 0.0), axis=0, keepdims=True)

    @pl.loop(0, n)
    def _(g):
        @pl.when(g != me)
        def _():
            qx.arrived(g)

        guarded(mix, g)

        @pl.when(g != me)
        def _():
            px.to(g).start()

        @pl.when(g == me)
        def _():
            p_recv[me] = p_send[g]

    fetch[11].wait()
    px.wait_recv()
    mixed = p_recv[0]
    for e in range(1, n):
        mixed = mixed + p_recv[e]
    for h in range(heads):
        own = jnp.sum(qk[:, h * kc:(h + 1) * kc], axis=1, keepdims=True)
        part = slice(h * dv, (h + 1) * dv)
        x = mixed[:, part] + own * fresh_value[:, part]
        mean_sq = jnp.mean(x * x, axis=1, keepdims=True)
        v = outgate[:, part]
        gated = x * lax.rsqrt(mean_sq + NORM_EPSILON) * hgain[...] * (v / (1.0 + jnp.exp(-v)))
        g_own[:, part] = gated
    gx.start()
    g_recv[me] = g_own[...]
    fetch[12].wait()
    gx.wait_recv()
    for d in range(min(n, seqs // spd)):
        g_full[d * spd:(d + 1) * spd, :] = g_recv[d]
    o_own[...] = dot(g_full[...].astype(BF16), wout[...]).astype(BF16)
    ox.start()
    o_recv[mt] = o_own[...]
    fetch[13].wait()
    fetch[14].wait()
    ox.wait_recv()
    attn = o_recv[0].astype(F32)
    for e in range(1, m):
        attn = attn + o_recv[e].astype(F32)
    residual = rows_float + attn

    s_own[...] = jnp.broadcast_to(jnp.sum(residual * residual, axis=1, keepdims=True), s_own.shape)
    sx.start()
    s_recv[me] = s_own[...]
    scaled_two = (residual * gain2[...]).astype(BF16)
    fetch[15].wait()
    for d in range(pl.cdiv(hidden, hw)):
        lo, size = d * hw, min(hw, hidden - d * hw)
        e_send[d, 0:seqs, 0:size] = dot(scaled_two, wg[:, lo:lo + size]).astype(BF16)
        e_send[d, seqs:2 * seqs, 0:size] = dot(scaled_two, wu[:, lo:lo + size]).astype(BF16)
    ex.start()
    e_recv[me] = e_send[me]
    sx.wait_recv()
    sq = s_recv[0]
    for e in range(1, n):
        sq = sq + s_recv[e]
    inv_two = lax.rsqrt(sq[:, 0:1] / model + NORM_EPSILON)
    fetch[16].wait()
    ex.wait_recv()
    both = e_recv[0].astype(F32)
    for e in range(1, n):
        both = both + e_recv[e].astype(F32)
    gate = inv_two * both[0:seqs]
    up = inv_two * both[seqs:2 * seqs]
    h_own[...] = (gate / (1.0 + jnp.exp(-gate)) * up).astype(BF16)
    hx.start()
    h_recv[me] = h_own[...]
    hx.wait_recv()
    down = jnp.zeros((seqs, width), F32)
    for d in range(pl.cdiv(hidden, hw)):
        lo, size = d * hw, min(hw, hidden - d * hw)
        down = down + dot(h_recv[d, :, 0:size], wd[lo:lo + size, :])
    f_own[...] = down.astype(BF16)
    fx.start()
    f_recv[mt] = f_own[...]
    for x in (ax, tx, qx, px, gx, sx, ex, hx, ox):
        x.wait_send()
    fx.wait_recv()
    result = residual
    for e in range(m):
        result = result + f_recv[e].astype(F32)
    out_ref[...] = result.astype(BF16)
    fx.wait_send()


def solution(mesh):
    n, m = mesh.shape["kv"], mesh.shape["tp"]

    def shards(
        tokens, attention_norm_gain, query_weight, key_weight, value_weight, output_gate_weight,
        lowrank_weight, decay_weight, decay_preact_bias, head_norm_gain, output_weight,
        feedforward_norm_gain, feedforward_gate_weight, feedforward_up_weight,
        feedforward_down_weight, past_key_cache, past_value_cache, past_lowrank_cache,
        head_extra_decay, lengths,
    ):
        seqs, width = tokens.shape
        chans, vals = query_weight.shape[1], value_weight.shape[1]
        positions = past_key_cache.shape[1]
        rank = lowrank_weight.shape[1]
        hidden = feedforward_gate_weight.shape[1]
        spd = pl.cdiv(seqs, n)
        hw = pl.cdiv(pl.cdiv(hidden, LANES), n) * LANES
        acols = 2 * chans + 2 * vals + 2 * LANES
        V = pltpu.VMEM

        def like(a):
            return V(a.shape, a.dtype)

        args = (
            tokens, attention_norm_gain[None], query_weight, key_weight, value_weight,
            output_gate_weight, lowrank_weight, decay_weight, decay_preact_bias[None],
            head_norm_gain[None], output_weight, feedforward_norm_gain[None],
            feedforward_gate_weight, feedforward_up_weight, feedforward_down_weight,
            past_key_cache, past_value_cache, past_lowrank_cache, head_extra_decay, lengths,
        )
        scratch = [
            like(tokens), V((1, width), F32), like(query_weight), like(key_weight),
            like(value_weight), like(output_gate_weight), V((width, rank), BF16),
            V((rank, chans), BF16), V((1, chans), F32), V((1, head_norm_gain.shape[0]), F32),
            like(output_weight), V((1, width), F32), like(feedforward_gate_weight),
            like(feedforward_up_weight), like(feedforward_down_weight), like(past_key_cache),
            like(past_value_cache), like(past_lowrank_cache), like(head_extra_decay),
            V((positions + 16, positions), BF16), V((positions, positions), BF16),
            V((seqs, 8, positions), F32), V((seqs, acols), F32),
            V((n, spd, acols), F32), V((n, spd, acols), F32),
            V((n, spd, chans), F32), V((n, spd, chans), F32),
            V((n, spd, chans), F32), V((n, spd, chans), F32),
            V((n, spd, vals), F32), V((n, spd, vals), F32),
            V((spd, vals), F32), V((n, spd, vals), F32), V((seqs, vals), F32),
            V((seqs, width), BF16), V((m, seqs, width), BF16),
            V((seqs, LANES), F32), V((n, seqs, LANES), F32),
            V((n, 2 * seqs, hw), BF16), V((n, 2 * seqs, hw), BF16),
            V((seqs, hw), BF16), V((n, seqs, hw), BF16),
            V((seqs, width), BF16), V((m, seqs, width), BF16),
            pltpu.SemaphoreType.DMA((17,)), pltpu.SemaphoreType.DMA((seqs,)),
            pltpu.SemaphoreType.DMA((seqs,)),
            pltpu.SemaphoreType.DMA((8, n)), pltpu.SemaphoreType.DMA((8, n)),
            pltpu.SemaphoreType.DMA((2, m)), pltpu.SemaphoreType.DMA((2, m)),
        ]
        specs = [pl.BlockSpec(memory_space=pl.ANY)] * (len(args) - 1)
        specs.append(pl.BlockSpec(memory_space=pltpu.SMEM))
        return pl.pallas_call(
            functools.partial(layer, n, m, spd),
            out_shape=jax.ShapeDtypeStruct((seqs, width), BF16),
            in_specs=specs,
            out_specs=pl.BlockSpec(memory_space=V),
            scratch_shapes=scratch,
            compiler_params=pltpu.CompilerParams(
                collective_id=0, has_side_effects=True, vmem_limit_bytes=64_000_000
            ),
        )(*args)

    return jax.shard_map(
        shards,
        mesh=mesh,
        in_specs=(
            P(None, "kv"), P(), P("kv", "tp"), P("kv", "tp"), P("kv", "tp"), P("kv", "tp"),
            P(), P(), P(), P(), P("tp", "kv"), P(), P("kv", "tp"), P("kv", "tp"),
            P("tp", "kv"), P(None, "kv", "tp"), P(None, "kv", "tp"), P(None, None, "kv"),
            P(None, "tp", "kv"), P(),
        ),
        out_specs=P(None, "kv"),
        check_vma=False,
    )
```

time: 304 us -> 69.4 us (0.23)
  waiting for transfers between devices: 95 us -> 0 us
  Pallas kernels: 0 us -> 65.6 us
  blocking collectives: 63.3 us -> 0 us
  local copies, waits for them, and re-layouts: 53.1 us -> 3.59 us
  matrix products: 45.8 us -> 0 us
  other arithmetic: 31.8 us -> 0 us
  between operations: 13.4 us -> 0.01 us
    psum x3 -> x0, waiting for transfers between devices: 95 us -> none  [the longest x2 53.7 us: shards(): lax.psum((jnp.sum(rows_float * rows_float, axis=1), product(scaled, query...]
    pallas_call x0 -> x1, Pallas kernels: none -> 65.6 us  [shards(): pl.pallas_call(functools.partial(layer, n, m, spd), out_shape=jax.ShapeDt...]
    psum x3 -> x0, blocking collectives: 47 us -> none  [the longest x1 16.8 us: shards(): lax.psum(product(gated.reshape(sequences, device_heads * DV), output_weig...]
    dot_general x14 -> x0, matrix products: 45.8 us -> none  [the longest x10 15.9 us: product(): return jnp.dot(operand, weights, preferred_element_type=jnp.float32)]
    add x3 -> x0, local copies, waits for them, and re-layouts: 32.2 us -> none  [shards(): gate_cache.reshape(sequences, positions, device_heads, KEY_CHANNELS)]
    all_gather x1 -> x0, blocking collectives: 16.3 us -> none  [shards(): pieces = lax.all_gather(local_total[:, None, :], 'kv', axis=1, tiled=True)]
    reduce_sum x7 -> x0, other arithmetic: 15.3 us -> none  [the longest x1 9.88 us: shards(): jnp.sum(products.reshape(sequences, positions, device_heads, KEY_CHANNELS...]
    reshape x4 -> x0, local copies, waits for them, and re-layouts: 12 us -> none  [the longest x1 11.9 us: shards(): products.reshape(sequences, positions, device_heads, KEY_CHANNELS)]
  transfers between devices with their start and end apart: 3 -> 0, of which waited for: 2 -> 0; matrix products, arithmetic and copies ran while one was open for 17% -> 0% of each run, Pallas kernels for 0% -> 0%
where the time goes in v1:
time: 69.4 us; the launch traced here: 69.2 us
  Pallas kernels  65.6 us (95%)
  local copies, waits for them, and re-layouts  3.59 us (5%)
    pallas_call x1, Pallas kernels, shards(): pl.pallas_call(functools.partial(layer, n, m, spd), out_shape=jax.ShapeDt...  65.6 us
    unnamed x2, local copies, waits for them, and re-layouts  3.59 us

profile of v1, /device:TPU:0, one launch (start us, length us, event | category | flops | bytes accessed | tf_op | source)
XLA Modules:
  0.0 69.2 jit_solution(231620253078562834)
XLA Ops:
  0.0 2.2 %copy.21.low_h = bf16[4096,16]{1,0:T(8,128)(2,1)} copy(bf16[4096,16]{0,1:T(8,128)(2,1)} %param.26) | data formatting | bytes 262144 | tf_op args[6]
  2.2 65.6 %shard_map.190 = bf16[24,512]{1,0:T(8,128)(2,1)} custom-call(bf16[24,512]{1,0:T(8,128)(2,1)} %tokens_h.1, f32[1,4096]{1,0:T(1,128)} %bitcast.4, bf16[512,512]{1,0:T(8,128)(2,1)} %wq_h.1, bf16[512,512]{1,0:T(8,128)(2,1)} %wk_h.1, bf16[512,1024]{1,0:T(8,128)(2,1)} %wv_h.1, bf16[512,1024]{1,0:T(8,128)(2,1)} %wo_h.1, bf16[4096,16]{1,0:T(8,128)(2,1)} %copy.21.low_h, ...), custom_call_target="tpu_custom_call" | custom-call | tf_op jit(solution)/shard_map/pallas_call | solution.py:420
  67.8 1.3 %copy.23 = bf16[24,512]{1,0:T(8,128)(2,1)} copy(bf16[24,512]{1,0:T(8,128)(2,1)} %shard_map.190) | data formatting | bytes 49152

commit v2 on v1

--- a/solution.py
+++ b/solution.py
@@ -76,8 +76,8 @@
     key, val, lr, ext,
     tri, tri_t, efac, a_full, a_send, a_recv, t_send, t_recv, q_send, q_recv,
     p_send, p_recv, g_own, g_recv, g_full, o_own, o_recv, s_own, s_recv,
-    e_send, e_recv, h_own, h_recv, f_own, f_recv,
-    in_sem, key_sem, val_sem, kv_ss, kv_rs, tp_ss, tp_rs,
+    u_send, u_recv, e_send, e_recv, h_own, h_recv, f_own, f_recv,
+    in_sem, key_sem, val_sem, kv_ss, kv_rs, tp_ss, tp_rs, u_ss, u_rs,
 ):
     me = lax.axis_index("kv")
     mt = lax.axis_index("tp")
@@ -85,13 +85,10 @@
     chans, vals = wq.shape[1], wv.shape[1]
     heads, positions = ext.shape[1], ext.shape[2]
     kc, dv = chans // heads, vals // heads
-    rank = low.shape[1]
+    rank = low.shape[0]
     hidden = wg.shape[1]
     hw = e_send.shape[2]
     model = width * n
-
-    def rows_of(ref, start, size):
-        return ref.at[pl.ds(pl.multiple_of(start, size), size)]
 
     def cols_of(ref, start, size):
         return ref.at[:, pl.ds(pl.multiple_of(start, size), size)]
@@ -100,7 +97,7 @@
         (tokens_h, tokens),
         (cols_of(gain1_h, me * width, width), gain1),
         (wq_h, wq), (wk_h, wk), (wv_h, wv), (wo_h, wo),
-        (rows_of(low_h, me * width, width), low),
+        (cols_of(low_h, me * width, width), low),
         (cols_of(dw_h, mt * chans, chans), dw),
         (cols_of(bias_h, mt * chans, chans), bias),
         (lr_h, lr), (ext_h, ext),
@@ -145,8 +142,21 @@
     px = kv_exchange(3, p_send, p_recv)
     gx = kv_exchange(4, g_own, g_recv, True)
     sx = kv_exchange(5, s_own, s_recv, True)
-    ex = kv_exchange(6, e_send, e_recv)
-    hx = kv_exchange(7, h_own, h_recv, True)
+    zs = n // 2
+    z, core = lax.div(me, 2), lax.rem(me, 2)
+    partner = me + 1 - 2 * core
+
+    def u_copy(zc):
+        return remote(u_send.at[2 * zc + 1 - core], u_recv.at[zc], u_ss.at[zc], u_rs.at[zc], "kv", partner)
+
+    def e_copy(zc, slot):
+        return remote(
+            e_send.at[zc], e_recv.at[slot], kv_ss.at[6, zc], kv_rs.at[6, slot], "kv", 2 * zc + core
+        )
+
+    def h_copy(src, slot, send, dest):
+        return remote(src, h_recv.at[slot], kv_ss.at[7, send], kv_rs.at[7, slot], "kv", dest)
+
     ox = tp_exchange(0, o_own, o_recv)
     fx = tp_exchange(1, f_own, f_recv)
 
@@ -171,12 +181,14 @@
     low_at, sq_at = base, base + LANES
     fetch[6].wait()
     a_full[:, low_at:low_at + LANES] = jnp.zeros((seqs, LANES), F32)
-    a_full[:, low_at:low_at + rank] = dot(scaled, low[...])
+    a_full[:, low_at:low_at + rank] = lax.dot_general(
+        scaled, low[...], (((1,), (1,)), ((), ())), preferred_element_type=F32
+    )
     a_full[:, sq_at:sq_at + LANES] = jnp.broadcast_to(
         jnp.sum(rows_float * rows_float, axis=1, keepdims=True), (seqs, LANES)
     )
     for d in range(min(n, seqs // spd)):
-        a_send[d] = a_full[d * spd:(d + 1) * spd, :]
+        a_send[d] = a_full[d * spd:(d + 1) * spd, :].astype(BF16)
     pl.semaphore_wait(barrier, n + m - 2)
     ax.start()
     a_recv[me] = a_send[me]
@@ -234,9 +246,9 @@
             t_recv[me] = t_send[g]
 
     ax.wait_recv()
-    total = a_recv[0]
+    total = a_recv[0].astype(F32)
     for e in range(1, n):
-        total = total + a_recv[e]
+        total = total + a_recv[e].astype(F32)
     inv = lax.rsqrt(total[:, sq_at:sq_at + 1] / model + NORM_EPSILON)
 
     def rounded(start, size):
@@ -299,13 +311,13 @@
         mean_sq = jnp.mean(x * x, axis=1, keepdims=True)
         v = outgate[:, part]
         gated = x * lax.rsqrt(mean_sq + NORM_EPSILON) * hgain[...] * (v / (1.0 + jnp.exp(-v)))
-        g_own[:, part] = gated
+        g_own[:, part] = gated.astype(BF16)
     gx.start()
     g_recv[me] = g_own[...]
     fetch[12].wait()
     gx.wait_recv()
     for d in range(min(n, seqs // spd)):
-        g_full[d * spd:(d + 1) * spd, :] = g_recv[d]
+        g_full[d * spd:(d + 1) * spd, :] = g_recv[d].astype(F32)
     o_own[...] = dot(g_full[...].astype(BF16), wout[...]).astype(BF16)
     ox.start()
     o_recv[mt] = o_own[...]
@@ -322,28 +334,50 @@
     s_recv[me] = s_own[...]
     scaled_two = (residual * gain2[...]).astype(BF16)
     fetch[15].wait()
-    for d in range(pl.cdiv(hidden, hw)):
+    for d in range(n):
         lo, size = d * hw, min(hw, hidden - d * hw)
-        e_send[d, 0:seqs, 0:size] = dot(scaled_two, wg[:, lo:lo + size]).astype(BF16)
-        e_send[d, seqs:2 * seqs, 0:size] = dot(scaled_two, wu[:, lo:lo + size]).astype(BF16)
-    ex.start()
-    e_recv[me] = e_send[me]
+        if size > 0:
+            u_send[d, 0:seqs, 0:size] = dot(scaled_two, wg[:, lo:lo + size]).astype(BF16)
+            u_send[d, seqs:2 * seqs, 0:size] = dot(scaled_two, wu[:, lo:lo + size]).astype(BF16)
+        if d % 2:
+            u_copy(d // 2).start()
+    for k in range(1, zs + 1):
+        zc = lax.rem(z + k, zs)
+        u_copy(zc).wait_recv()
+        pair = u_send[2 * zc + core].astype(F32) + u_recv[zc].astype(F32)
+        if k < zs:
+            e_send[zc] = pair.astype(BF16)
+            e_copy(zc, z).start()
+        else:
+            e_recv[z] = pair.astype(BF16)
     sx.wait_recv()
     sq = s_recv[0]
     for e in range(1, n):
         sq = sq + s_recv[e]
     inv_two = lax.rsqrt(sq[:, 0:1] / model + NORM_EPSILON)
     fetch[16].wait()
-    ex.wait_recv()
+    for k in range(1, zs):
+        zc = lax.rem(z + k, zs)
+        e_copy(zc, zc).wait_recv()
     both = e_recv[0].astype(F32)
-    for e in range(1, n):
+    for e in range(1, zs):
         both = both + e_recv[e].astype(F32)
     gate = inv_two * both[0:seqs]
     up = inv_two * both[seqs:2 * seqs]
     h_own[...] = (gate / (1.0 + jnp.exp(-gate)) * up).astype(BF16)
-    hx.start()
+    for k in range(1, zs):
+        dest = 2 * lax.rem(z + k, zs) + core
+        h_copy(h_own, me, dest, dest).start()
+    h_copy(h_own, me, partner, partner).start()
     h_recv[me] = h_own[...]
-    hx.wait_recv()
+    for k in range(1, zs):
+        zc = lax.rem(z + k, zs)
+        origin = 2 * zc + core
+        h_copy(h_own, origin, origin, origin).wait_recv()
+        h_copy(h_recv.at[origin], origin, 2 * zc + 1 - core, partner).start()
+    for k in range(zs):
+        origin = 2 * lax.rem(z + k, zs) + 1 - core
+        h_copy(h_own, origin, origin, partner).wait_recv()
     down = jnp.zeros((seqs, width), F32)
     for d in range(pl.cdiv(hidden, hw)):
         lo, size = d * hw, min(hw, hidden - d * hw)
@@ -351,8 +385,15 @@
     f_own[...] = down.astype(BF16)
     fx.start()
     f_recv[mt] = f_own[...]
-    for x in (ax, tx, qx, px, gx, sx, ex, hx, ox):
+    for x in (ax, tx, qx, px, gx, sx, ox):
         x.wait_send()
+    for k in range(zs):
+        zc = lax.rem(z + k, zs)
+        u_copy(zc).wait_send()
+        h_copy(h_own, me, 2 * zc + 1 - core, partner).wait_send()
+        if k > 0:
+            e_copy(zc, z).wait_send()
+            h_copy(h_own, me, 2 * zc + core, partner).wait_send()
     fx.wait_recv()
     result = residual
     for e in range(m):
@@ -386,34 +427,36 @@
 
         args = (
             tokens, attention_norm_gain[None], query_weight, key_weight, value_weight,
-            output_gate_weight, lowrank_weight, decay_weight, decay_preact_bias[None],
+            output_gate_weight, lowrank_weight.T, decay_weight, decay_preact_bias[None],
             head_norm_gain[None], output_weight, feedforward_norm_gain[None],
             feedforward_gate_weight, feedforward_up_weight, feedforward_down_weight,
             past_key_cache, past_value_cache, past_lowrank_cache, head_extra_decay, lengths,
         )
         scratch = [
             like(tokens), V((1, width), F32), like(query_weight), like(key_weight),
-            like(value_weight), like(output_gate_weight), V((width, rank), BF16),
+            like(value_weight), like(output_gate_weight), V((rank, width), BF16),
             V((rank, chans), BF16), V((1, chans), F32), V((1, head_norm_gain.shape[0]), F32),
             like(output_weight), V((1, width), F32), like(feedforward_gate_weight),
             like(feedforward_up_weight), like(feedforward_down_weight), like(past_key_cache),
             like(past_value_cache), like(past_lowrank_cache), like(head_extra_decay),
             V((positions + 16, positions), BF16), V((positions, positions), BF16),
             V((seqs, 8, positions), F32), V((seqs, acols), F32),
-            V((n, spd, acols), F32), V((n, spd, acols), F32),
+            V((n, spd, acols), BF16), V((n, spd, acols), BF16),
             V((n, spd, chans), F32), V((n, spd, chans), F32),
             V((n, spd, chans), F32), V((n, spd, chans), F32),
             V((n, spd, vals), F32), V((n, spd, vals), F32),
-            V((spd, vals), F32), V((n, spd, vals), F32), V((seqs, vals), F32),
+            V((spd, vals), BF16), V((n, spd, vals), BF16), V((seqs, vals), F32),
             V((seqs, width), BF16), V((m, seqs, width), BF16),
             V((seqs, LANES), F32), V((n, seqs, LANES), F32),
-            V((n, 2 * seqs, hw), BF16), V((n, 2 * seqs, hw), BF16),
+            V((n, 2 * seqs, hw), BF16), V((n // 2, 2 * seqs, hw), BF16),
+            V((n // 2, 2 * seqs, hw), BF16), V((n // 2, 2 * seqs, hw), BF16),
             V((seqs, hw), BF16), V((n, seqs, hw), BF16),
             V((seqs, width), BF16), V((m, seqs, width), BF16),
             pltpu.SemaphoreType.DMA((17,)), pltpu.SemaphoreType.DMA((seqs,)),
             pltpu.SemaphoreType.DMA((seqs,)),
             pltpu.SemaphoreType.DMA((8, n)), pltpu.SemaphoreType.DMA((8, n)),
             pltpu.SemaphoreType.DMA((2, m)), pltpu.SemaphoreType.DMA((2, m)),
+            pltpu.SemaphoreType.DMA((n // 2,)), pltpu.SemaphoreType.DMA((n // 2,)),
         ]
         specs = [pl.BlockSpec(memory_space=pl.ANY)] * (len(args) - 1)
         specs.append(pl.BlockSpec(memory_space=pltpu.SMEM))

time: 69.4 us -> 64 us (0.922)
  Pallas kernels: 65.6 us -> 62.4 us
  local copies, waits for them, and re-layouts: 3.59 us -> 1.35 us
    pallas_call x1, Pallas kernels: 65.6 us -> 62.4 us  [shards(): pl.pallas_call(functools.partial(layer, n, m, spd), out_shape=jax.ShapeDt...]
    unnamed x2 -> x1, local copies, waits for them, and re-layouts: 3.59 us -> 1.35 us
where the time goes in v2:
time: 64 us; the launch traced here: 63.8 us
  Pallas kernels  62.4 us (98%)
  local copies, waits for them, and re-layouts  1.35 us (2%)
    pallas_call x1, Pallas kernels, shards(): pl.pallas_call(functools.partial(layer, n, m, spd), out_shape=jax.ShapeDt...  62.4 us
    unnamed x1, local copies, waits for them, and re-layouts  1.35 us

profile of v2, /device:TPU:0, one launch (start us, length us, event | category | flops | bytes accessed | tf_op | source)
XLA Modules:
  0.0 63.8 jit_solution(1050099444353545081)
XLA Ops:
  0.0 62.4 %shard_map.190 = bf16[24,512]{1,0:T(8,128)(2,1)} custom-call(bf16[24,512]{1,0:T(8,128)(2,1)} %tokens_h.1, f32[1,4096]{1,0:T(1,128)} %bitcast.6, bf16[512,512]{1,0:T(8,128)(2,1)} %wq_h.1, bf16[512,512]{1,0:T(8,128)(2,1)} %wk_h.1, bf16[512,1024]{1,0:T(8,128)(2,1)} %wv_h.1, bf16[512,1024]{1,0:T(8,128)(2,1)} %wo_h.1, bf16[16,4096]{1,0:T(8,128)(2,1)} %bitcast.5, ...), custom_call_target="tpu_custom_call" | custom-call | tf_op jit(solution)/shard_map/pallas_call | solution.py:463
  62.4 1.3 %copy.22 = bf16[24,512]{1,0:T(8,128)(2,1)} copy(bf16[24,512]{1,0:T(8,128)(2,1)} %shard_map.190) | data formatting | bytes 49152
